TPU v7x, 512 devices: a 4x2x32 block of a 4x8x32 slice. The times are simulated.
512 devices in a mesh: grp: 2 (over y), fs: 32 (over z), tp: 8 (over x, core).
Axes of the slice: x: 4, y: 2, z: 32, core: 2. Of those that a mesh axis runs over, the one named last changes fastest.
The devices are a block of a 4x8x32 slice.
Arguments:
- stream: bfloat16 [64, 128, 2048], P(('grp', 'fs')), parts along dimension 0, may hold values from -6 to 6
- in_gain: float32 [2048], replicated, may hold values from 0.2 to 5
- value_weight: bfloat16 [2048, 1024], P('fs', 'tp'), may hold values from -0.125 to 0.125
- gate_weight: bfloat16 [2048, 1024], P('fs', 'tp'), may hold values from -0.125 to 0.125
- conv_kernel: bfloat16 [31, 1024], P(None, 'tp'), may hold values from -3.6 to 3.6
- conv_gain: float32 [1024], P('tp'), may hold values from 0.1 to 1.9
- conv_shift: float32 [1024], P('tp'), may hold values from -3 to 3
- out_weight: bfloat16 [1024, 2048], P('tp', 'fs'), may hold values from -0.1875 to 0.1875
- norm_gain: float32 [2048], replicated, may hold values from 0.2 to 5
- up_weight: bfloat16 [2048, 8192], P('fs', 'tp'), may hold values from -0.125 to 0.125
- down_weight: bfloat16 [8192, 2048], P('tp', 'fs'), may hold values from -0.0625 to 0.0625
- out_gain: float32 [2048], P('tp'), may hold values from 0.1 to 1.9
Outputs:
- result: bfloat16 [64, 128, 2048], P(('grp', 'fs'), None, 'tp'), parts along dimension 0
There are 2 independent parts, one for each index of `grp`. A program takes and returns all parts, laid end to end along the dimension named above; an argument that names none is the same for every part. Nothing has to cross between parts.
All inputs are finite; a program needn't handle non-finite values.
Results may differ from a plain program's by a relative error of at most 0.02.
Values may be sent and summed in bfloat16 or wider, within the bound.
No kernel may reach another device: no remote copies, remote signals or barrier semaphores. Data moves between devices by JAX's collectives and lax.ppermute only.
A program may use at most 64 MiB of HBM per device.

v0:
```python
import jax
import jax.numpy as jnp
from jax import lax
from jax.sharding import PartitionSpec as P

KW = 31
norm_epsilon = 1e-05
residual_scale = 2.0**0.25


def gather_fs(x):
    groups = lax.axis_size("grp")
    rows = x.shape[0] // groups
    own = lax.dynamic_slice_in_dim(x, lax.axis_index("grp") * rows, rows, 0)
    return lax.all_gather(own, ("fs", "grp"), axis=0, tiled=True)


def norm_rows(values, gain_vector):
    row_mean = jnp.mean(values, axis=-1, keepdims=True)
    row_var = jnp.mean(jnp.square(values - row_mean), axis=-1, keepdims=True)
    return (values - row_mean) * lax.rsqrt(row_var + norm_epsilon) * gain_vector


def contract(left, turned):
    return lax.dot_general(
        left, turned, (((1,), (1,)), ((), ())), preferred_element_type=jnp.float32
    )


def swap_blocks(x):
    return lax.all_to_all(x, "tp", 0, 0, tiled=True)


def summed_tokens(terms):
    tp_count = lax.axis_size("tp")
    tokens, width = terms.shape
    tiles = swap_blocks(terms.astype(jnp.bfloat16).reshape(tp_count, tokens // tp_count, width))
    return jnp.sum(tiles.astype(jnp.float32), axis=0).astype(jnp.bfloat16)


def shards(
    stream,
    in_gain,
    value_weight,
    gate_weight,
    conv_kernel,
    conv_gain,
    conv_shift,
    out_weight,
    norm_gain,
    up_weight,
    down_weight,
    out_gain,
):
    seq_count, seq_length, model_width = stream.shape
    token_count = seq_count * seq_length
    tp_count = lax.axis_size("tp")
    slice_width = model_width // tp_count
    own_tokens = token_count // tp_count
    tp_index = lax.axis_index("tp")
    channels = value_weight.shape[1]
    first = gather_fs(jnp.concatenate([value_weight, gate_weight, out_weight.T], axis=1))
    up_weight, first = lax.optimization_barrier((up_weight, first))
    up_whole = gather_fs(up_weight)
    down_weight, up_whole = lax.optimization_barrier((down_weight, up_whole))
    down_turned = gather_fs(down_weight.T)
    value_gate, out_turned = (first[:, : 2 * channels], first[:, 2 * channels :])
    normed = norm_rows(
        stream.reshape(token_count, model_width).astype(jnp.float32), in_gain
    ).astype(jnp.bfloat16)
    both = jnp.dot(normed, value_gate, preferred_element_type=jnp.float32)
    gated = (both[:, :channels] * jax.nn.sigmoid(both[:, channels:])).astype(jnp.bfloat16)
    convolved = lax.conv_general_dilated(
        gated.reshape(seq_count, seq_length, channels),
        conv_kernel[:, None, :],
        window_strides=(1,),
        padding=[(KW - 1, 0)],
        dimension_numbers=("NWC", "WIO", "NWC"),
        feature_group_count=channels,
        preferred_element_type=jnp.float32,
    ).reshape(token_count, channels)
    sums = jnp.stack([jnp.sum(convolved, axis=1), jnp.sum(convolved * convolved, axis=1)])
    sums = jnp.sum(swap_blocks(jnp.broadcast_to(sums[None], (tp_count, *sums.shape))), axis=0)
    row_mean = sums[0] / (channels * tp_count)
    row_var = sums[1] / (channels * tp_count) - row_mean * row_mean
    activated = jax.nn.silu(
        (convolved - row_mean[:, None]) * lax.rsqrt(row_var + norm_epsilon)[:, None] * conv_gain
        + conv_shift
    ).astype(jnp.bfloat16)
    mixed = summed_tokens(contract(activated, out_turned))
    normed_own = lax.dynamic_slice_in_dim(normed, tp_index * own_tokens, own_tokens, 0)
    settled_own = norm_rows(
        residual_scale * normed_own.astype(jnp.float32) + mixed.astype(jnp.float32), norm_gain
    ).astype(jnp.bfloat16)
    settled = lax.all_gather(settled_own, "tp", axis=0, tiled=True)
    whole_gain = lax.all_gather(out_gain, "tp", axis=0, tiled=True)
    hidden = jnp.square(
        jax.nn.relu(jnp.dot(settled, up_whole, preferred_element_type=jnp.float32))
    ).astype(jnp.bfloat16)
    fed = summed_tokens(contract(hidden, down_turned))
    result_own = norm_rows(
        residual_scale * settled_own.astype(jnp.float32) + fed.astype(jnp.float32), whole_gain
    ).astype(jnp.bfloat16)
    pieces = jnp.moveaxis(result_own.reshape(own_tokens, tp_count, slice_width), 1, 0)
    result = swap_blocks(pieces)
    return result.reshape(seq_count, seq_length, slice_width)


def solution(mesh):
    in_specs = (
        P(("grp", "fs"), None, None),
        P(),
        P("fs", "tp"),
        P("fs", "tp"),
        P(None, "tp"),
        P("tp"),
        P("tp"),
        P("tp", "fs"),
        P(),
        P("fs", "tp"),
        P("tp", "fs"),
        P("tp"),
    )
    out_specs = P(("grp", "fs"), None, "tp")
    return jax.shard_map(shards, mesh=mesh, in_specs=in_specs, out_specs=out_specs, check_vma=False)
```

profile of v0, /device:TPU:33, one launch (start us, length us, event | category | flops | bytes accessed | tf_op | source)
XLA Modules:
  0.0 904.0 jit_solution(4344918902688362367)
XLA Ops:
  6.5 0.0 copy-start
  6.6 0.0 copy-start.5
  6.6 0.0 copy-start.4
  6.6 0.0 copy-start.3
  6.6 0.1 all-gather.5.cloned.1.call-start
  6.6 1.4 fusion.28
  8.0 0.1 all-gather.5.cloned.1.call-update
  8.1 0.1 all-gather.7.cloned.1.call-start
  8.1 277.9 %all-gather.5.cloned.1.call-done = bf16[2048,384]{1,0:T(8,128)(2,1)} async-done(((bf16[32,384]{1,0:T(8,128)(2,1)}), bf16[2048,384]{1,0:T(8,128)(2,1)}) %all-gather.5.cloned.1.call-update) | async-done | bytes 1572880 | tf_op jit(solution)/shard_map/all_gather | solution.py:15
  286.0 0.0 copy-done
  286.0 0.6 constant_dynamic-slice_fusion
  286.7 0.1 all-gather.7.cloned.1.call-update
  286.7 0.1 all-gather.9.cloned.1.call-start
  286.8 278.4 %all-gather.7.cloned.1.call-done = bf16[2048,1024]{1,0:T(8,128)(2,1)} async-done(((bf16[32,1024]{1,0:T(8,128)(2,1)}), bf16[2048,1024]{1,0:T(8,128)(2,1)}) %all-gather.7.cloned.1.call-update) | async-done | bytes 4194320 | tf_op jit(solution)/shard_map/all_gather | solution.py:15
  565.2 1.5 dynamic-slice_bitcast_fusion
  566.7 0.1 all-gather.9.cloned.1.call-update
  566.7 0.0 copy-start.1
  566.7 1.2 convert_reduce_fusion
  567.9 1.3 fusion.5
  569.3 1.4 fusion.7
  570.7 1.5 fusion.8
  572.3 0.0 copy-done.5
  572.3 1.1 fusion.34
  573.4 0.1 multiply_reduce_fusion.2
  573.5 28.9 %all_to_all.20 = f32[8,2,128]{2,1,0:T(2,128)S(1)} all-to-all(f32[8,2,128]{2,1,0:T(2,128)S(1)} %broadcast_in_dim.5), channel_id=1, replica_groups=mesh['grp'=2,'fs'=32,'tp'=8] {'tp'}, dimensions={0} | all-to-all | bytes 16384 | tf_op jit(solution)/shard_map/all_to_all | solution.py:31
  602.5 0.0 copy-done.4
  602.5 0.0 copy-done.3
  602.5 2.2 convolution_convert_fusion.1
  604.7 4.1 all-to-all-start.1
  608.8 9.4 %all-to-all-done.1 = bf16[8,16,2048]{2,1,0:T(8,128)(2,1)S(1)} async-done(((bf16[8,16,2048]{2,1,0:T(8,128)(2,1)}), bf16[8,16,2048]{2,1,0:T(8,128)(2,1)S(1)}, u32[]{:S(2)}, u32[]{:S(2)}) %all-to-all-start.1) | async-done | bytes 524320 | tf_op jit(solution)/shard_map/all_to_all | solution.py:31
  618.2 0.1 reduce_sum.110
  618.3 0.1 fusion.12
  618.5 0.2 multiply_reduce_fusion.1
  618.7 0.0 copy-done.1
  618.7 0.1 multiply_convert_fusion.1
  618.8 14.0 %all_gather.16 = bf16[128,2048]{1,0:T(8,128)(2,1)S(1)} all-gather(bf16[16,2048]{1,0:T(8,128)(2,1)S(1)} %multiply_convert_fusion.1), channel_id=1, replica_groups=mesh['grp'=2,'fs'=32,'tp'=8] {'tp'}, dimensions={0}, use_global_device_ids=true | all-gather | bytes 589824 | tf_op jit(solution)/shard_map/all_gather | solution.py:95
  632.8 0.0 copy-start.2
  632.8 211.7 %all-gather.9.cloned.1.call-done = bf16[2048,1024]{1,0:T(8,128)(2,1)} async-done(((bf16[32,1024]{1,0:T(8,128)(2,1)}), bf16[2048,1024]{1,0:T(8,128)(2,1)}) %all-gather.9.cloned.1.call-update) | async-done | bytes 4194320 | tf_op jit(solution)/shard_map/all_gather | solution.py:15
  844.5 6.4 convolution_convert_fusion
  850.8 24.9 %all-to-all-start.2 = ((bf16[8,16,2048]{2,1,0:T(8,128)(2,1)}), bf16[8,16,2048]{2,1,0:T(8,128)(2,1)S(1)}, u32[]{:S(2)}, u32[]{:S(2)}) async-start(bf16[8,16,2048]{2,1,0:T(8,128)(2,1)} %bitcast.11), calls=%async_computation.2 | async-start | bytes 1048576 | tf_op jit(solution)/shard_map/all_to_all | solution.py:31
  875.7 0.0 copy-done.2
  875.7 13.1 %all-gather = f32[8,1,256]{2,1,0:T(1,128)S(1)} all-gather(f32[1,1,256]{2,1,0:T(1,128)S(1)} %bitcast.57), channel_id=1, replica_groups=mesh['grp'=2,'fs'=32,'tp'=8] {'tp'}, dimensions={0}, use_global_device_ids=true | all-gather | bytes 9216 | tf_op jit(solution)/shard_map/all_gather | solution.py:96
  888.8 0.0 all-to-all-done.2
  888.8 0.1 reduce_sum.113
  888.9 0.1 fusion.13
  889.1 0.2 multiply_reduce_fusion
  889.3 0.1 multiply_convert_fusion
  889.4 7.4 all_to_all.21
  896.8 0.6 copy.41
  (13 shorter events, 0.1 us)
Async XLA Ops:
  6.5 279.5 %copy-start = (bf16[64,1024]{1,0:T(8,128)(2,1)S(1)}, bf16[64,1024]{1,0:T(8,128)(2,1)}, u32[]{:S(2)}) copy-start(bf16[64,1024]{1,0:T(8,128)(2,1)} %param.21) | copy-start | bytes 393220
  6.6 565.7 %copy-start.5 = (bf16[31,128]{1,0:T(8,128)(2,1)S(1)}, bf16[31,128]{1,0:T(8,128)(2,1)}, u32[]{:S(2)}) copy-start(bf16[31,128]{1,0:T(8,128)(2,1)} %param.16) | copy-start | bytes 23812
  6.6 595.9 %copy-start.4 = (f32[128]{0:T(128)S(1)}, f32[128]{0:T(128)}, u32[]{:S(2)}) copy-start(f32[128]{0:T(128)} %param.17) | copy-start | bytes 1540
  6.6 595.9 %copy-start.3 = (f32[128]{0:T(128)S(1)}, f32[128]{0:T(128)}, u32[]{:S(2)}) copy-start(f32[128]{0:T(128)} %param.18) | copy-start | bytes 1540
  6.6 279.5 %all-gather.5.cloned.1.call-start = ((), (), s32[]{:S(2)}) async-start(), calls=%async_computation.4 | async-start | bytes 1597440 | tf_op jit(solution)/shard_map/all_gather | solution.py:15
  8.1 557.1 %all-gather.7.cloned.1.call-start = ((), (), s32[]{:S(2)}) async-start(), calls=%async_computation.5 | async-start | bytes 4259840 | tf_op jit(solution)/shard_map/all_gather | solution.py:15
  286.7 557.7 %all-gather.9.cloned.1.call-start = ((), (), s32[]{:S(2)}) async-start(), calls=%async_computation.6 | async-start | bytes 4259840 | tf_op jit(solution)/shard_map/all_gather | solution.py:15
  566.7 52.0 %copy-start.1 = (f32[2048]{0:T(1024)S(1)}, f32[2048]{0:T(1024)}, u32[]{:S(2)}) copy-start(f32[2048]{0:T(1024)} %param.20) | copy-start | bytes 24580
  604.7 13.5 %all-to-all-start.1 = ((bf16[8,16,2048]{2,1,0:T(8,128)(2,1)}), bf16[8,16,2048]{2,1,0:T(8,128)(2,1)S(1)}, u32[]{:S(2)}, u32[]{:S(2)}) async-start(bf16[8,16,2048]{2,1,0:T(8,128)(2,1)} %bitcast.9), calls=%async_computation.1 | async-start | bytes 1048576 | tf_op jit(solution)/shard_map/all_to_all | solution.py:31
  632.8 243.0 %copy-start.2 = (f32[256]{0:T(256)S(1)}, f32[256]{0:T(256)}, u32[]{:S(2)}) copy-start(f32[256]{0:T(256)} %param.23) | copy-start | bytes 3076
  850.8 38.0 %all-to-all-start.2 = ((bf16[8,16,2048]{2,1,0:T(8,128)(2,1)}), bf16[8,16,2048]{2,1,0:T(8,128)(2,1)S(1)}, u32[]{:S(2)}, u32[]{:S(2)}) async-start(bf16[8,16,2048]{2,1,0:T(8,128)(2,1)} %bitcast.11), calls=%async_computation.2 | async-start | bytes 1048576 | tf_op jit(solution)/shard_map/all_to_all | solution.py:31
Sparse Core Ops, SparseCore 0:
  10.5 275.4 all-gather.4
  289.2 275.9 all-gather.6
  568.3 276.0 all-gather.8
where the time goes:
time: 905 us; the launch traced here: 904 us
  waiting for transfers between devices  778 us (86%)
  blocking collectives  63.5 us (7%)
  starting transfers between devices  29.2 us (3%)
  between operations  13.3 us (1%)
  matrix products  11.2 us (1%)
    all_gather x3, waiting for transfers between devices, gather_fs(): return lax.all_gather(own, ('fs', 'grp'), axis=0, tiled=True)  768 us
    all_to_all x2, blocking collectives, swap_blocks(): return lax.all_to_all(x, 'tp', 0, 0, tiled=True)  36.4 us
    all_to_all x2, starting transfers between devices, swap_blocks(): return lax.all_to_all(x, 'tp', 0, 0, tiled=True)  29 us
  transfers between devices with their start and end apart: 5, of which 4 were waited for; matrix products, arithmetic and copies ran while one was open for 1% of the time, Pallas kernels for 0%

commit v1 on v0

--- a/solution.py
+++ b/solution.py
@@ -12,7 +12,9 @@
     groups = lax.axis_size("grp")
     rows = x.shape[0] // groups
     own = lax.dynamic_slice_in_dim(x, lax.axis_index("grp") * rows, rows, 0)
-    return lax.all_gather(own, ("fs", "grp"), axis=0, tiled=True)
+    return jnp.concatenate(
+        lax.all_to_all(jnp.stack([own] * lax.axis_size(("fs", "grp"))), ("fs", "grp"), 0, 0), axis=0
+    )
 
 
 def norm_rows(values, gain_vector):

time: 905 us -> 1040 us (1.15)
  waiting for transfers between devices: 778 us -> 886 us
  starting transfers between devices: 29.2 us -> 99.2 us
  blocking collectives: 63.5 us -> 34.6 us
  between operations: 13.3 us -> 0.19 us
    all_to_all x0 -> x3, waiting for transfers between devices: none -> 872 us  [gather_fs(): lax.all_to_all(jnp.stack([own] * lax.axis_size(('fs', 'grp'))), ('fs', 'g...]
    all_gather x3 -> x0, waiting for transfers between devices: 768 us -> none  [gather_fs(): return lax.all_gather(own, ('fs', 'grp'), axis=0, tiled=True)]
    all_to_all x0 -> x3, starting transfers between devices: none -> 64.3 us  [gather_fs(): lax.all_to_all(jnp.stack([own] * lax.axis_size(('fs', 'grp'))), ('fs', 'g...]
    all_to_all x2 -> x1, blocking collectives: 36.4 us -> 7.45 us  [swap_blocks(): return lax.all_to_all(x, 'tp', 0, 0, tiled=True)]
    all_to_all x2 -> x3, starting transfers between devices: 29 us -> 34.9 us  [swap_blocks(): return lax.all_to_all(x, 'tp', 0, 0, tiled=True)]
  transfers between devices with their start and end apart: 5 -> 6, of which waited for: 4 -> 5; matrix products, arithmetic and copies ran while one was open for 1% -> 0% of each run, Pallas kernels for 0% -> 0%
where the time goes in v1:
time: 1040 us
  waiting for transfers between devices  886 us (85%)
  starting transfers between devices  99.2 us (10%)
  blocking collectives  34.6 us (3%)
    all_to_all x3, waiting for transfers between devices, gather_fs(): lax.all_to_all(jnp.stack([own] * lax.axis_size(('fs', 'grp'))), ('fs', 'g...  872 us
    all_to_all x3, starting transfers between devices, gather_fs(): lax.all_to_all(jnp.stack([own] * lax.axis_size(('fs', 'grp'))), ('fs', 'g...  64.3 us
    all_to_all x3, starting transfers between devices, swap_blocks(): return lax.all_to_all(x, 'tp', 0, 0, tiled=True)  34.9 us
  transfers between devices with their start and end apart: 6, of which 5 were waited for; matrix products, arithmetic and copies ran while one was open for 0% of the time, Pallas kernels for 0%

profile of v1, /device:TPU:33, one launch (start us, length us, event | category | flops | bytes accessed | tf_op | source)
XLA Modules:
  0.0 1039.5 jit_solution(9497518872053203041)
XLA Ops:
  0.0 0.0 copy-start
  0.0 0.0 copy-start.1
  0.0 0.0 copy-start.3
  0.0 0.8 fusion.28
  0.8 0.0 copy-start.8
  0.8 1.3 stack.12
  2.1 49.4 %all-to-all-start = ((bf16[64,32,384]{2,1,0:T(8,128)(2,1)}), bf16[64,32,384]{2,1,0:T(8,128)(2,1)S(1)}, u32[]{:S(2)}, u32[]{:S(2)}) async-start(bf16[64,32,384]{2,1,0:T(8,128)(2,1)} %stack.12), calls=%async_computation | async-start | bytes 3145728 | tf_op jit(solution)/shard_map/all_to_all | solution.py:16
  51.5 0.0 copy-done.1
  51.5 0.2 convert_reduce_fusion
  51.7 0.3 fusion.5
  52.0 0.0 copy-done.3
  52.0 0.4 fusion.7
  52.4 148.0 %all-to-all-done = bf16[64,32,384]{2,1,0:T(8,128)(2,1)S(1)} async-done(((bf16[64,32,384]{2,1,0:T(8,128)(2,1)}), bf16[64,32,384]{2,1,0:T(8,128)(2,1)S(1)}, u32[]{:S(2)}, u32[]{:S(2)}) %all-to-all-start) | async-done | bytes 1572896 | tf_op jit(solution)/shard_map/all_to_all | solution.py:16
  200.4 0.3 fusion.8
  200.8 0.0 copy-done.8
  200.8 1.1 fusion.34
  201.9 0.1 multiply_reduce_fusion.2
  202.0 0.6 broadcast_in_dim.5
  202.6 9.9 all-to-all-start.1
  212.5 0.0 copy-done
  212.5 4.6 all-to-all-done.1
  217.1 2.5 stack.16
  219.6 0.0 copy-start.6
  219.7 0.0 copy-start.7
  219.7 0.0 copy-start.2
  219.7 7.4 all-to-all-start.3
  227.1 0.0 copy-done.6
  227.1 0.0 copy-done.7
  227.1 1.2 convolution_convert_fusion.1
  228.4 368.4 %all-to-all-done.3 = bf16[64,32,1024]{2,1,0:T(8,128)(2,1)} async-done(((bf16[64,32,1024]{2,1,0:T(8,128)(2,1)}), bf16[64,32,1024]{2,1,0:T(8,128)(2,1)}, u32[]{:S(2)}, u32[]{:S(2)}) %all-to-all-start.3) | async-done | bytes 4194336 | tf_op jit(solution)/shard_map/all_to_all | solution.py:16
  596.7 12.8 %all-to-all-start.2 = ((bf16[8,16,2048]{2,1,0:T(8,128)(2,1)}), bf16[8,16,2048]{2,1,0:T(8,128)(2,1)S(1)}, u32[]{:S(2)}, u32[]{:S(2)}) async-start(bf16[8,16,2048]{2,1,0:T(8,128)(2,1)} %bitcast.10), calls=%async_computation.2 | async-start | bytes 1048576 | tf_op jit(solution)/shard_map/all_to_all | solution.py:33
  609.5 0.0 copy-done.2
  609.5 9.4 all-to-all-done.2
  618.9 2.5 stack.17
  621.4 0.0 copy-start.4
  621.4 7.4 all-to-all-start.4
  628.9 0.1 reduce_sum.110
  629.0 0.1 fusion.12
  629.1 0.2 multiply_reduce_fusion.1
  629.3 0.0 copy-done.4
  629.3 0.1 multiply_convert_fusion.1
  629.4 14.0 %all_gather.6 = bf16[128,2048]{1,0:T(8,128)(2,1)S(1)} all-gather(bf16[16,2048]{1,0:T(8,128)(2,1)S(1)} %multiply_convert_fusion.1), channel_id=1, replica_groups=mesh['grp'=2,'fs'=32,'tp'=8] {'tp'}, dimensions={0}, use_global_device_ids=true | all-gather | bytes 589824 | tf_op jit(solution)/shard_map/all_gather | solution.py:97
  643.4 355.7 %all-to-all-done.4 = bf16[64,32,1024]{2,1,0:T(8,128)(2,1)} async-done(((bf16[64,32,1024]{2,1,0:T(8,128)(2,1)}), bf16[64,32,1024]{2,1,0:T(8,128)(2,1)}, u32[]{:S(2)}, u32[]{:S(2)}) %all-to-all-start.4) | async-done | bytes 4194336 | tf_op jit(solution)/shard_map/all_to_all | solution.py:16
  999.1 0.0 copy-start.5
  999.1 6.4 convolution_convert_fusion
  1005.5 12.2 %all-to-all-start.5 = ((bf16[8,16,2048]{2,1,0:T(8,128)(2,1)}), bf16[8,16,2048]{2,1,0:T(8,128)(2,1)S(1)}, u32[]{:S(2)}, u32[]{:S(2)}) async-start(bf16[8,16,2048]{2,1,0:T(8,128)(2,1)} %bitcast.14), calls=%async_computation.5 | async-start | bytes 1048576 | tf_op jit(solution)/shard_map/all_to_all | solution.py:33
  1017.7 0.0 copy-done.5
  1017.7 13.2 %all-gather = f32[8,1,256]{2,1,0:T(1,128)S(1)} all-gather(f32[1,1,256]{2,1,0:T(1,128)S(1)} %bitcast.62), channel_id=1, replica_groups=mesh['grp'=2,'fs'=32,'tp'=8] {'tp'}, dimensions={0}, use_global_device_ids=true | all-gather | bytes 9216 | tf_op jit(solution)/shard_map/all_gather | solution.py:98
  1030.9 0.0 all-to-all-done.5
  1030.9 0.1 reduce_sum.113
  1031.0 0.1 fusion.13
  1031.1 0.2 multiply_reduce_fusion
  1031.3 0.1 multiply_convert_fusion
  1031.5 7.4 all_to_all.35
  1038.9 0.6 copy.41
  (14 shorter events, 0.1 us)
Async XLA Ops:
  0.0 212.5 %copy-start = (bf16[64,1024]{1,0:T(8,128)(2,1)S(1)}, bf16[64,1024]{1,0:T(8,128)(2,1)}, u32[]{:S(2)}) copy-start(bf16[64,1024]{1,0:T(8,128)(2,1)} %param.21) | copy-start | bytes 393220
  0.0 51.5 %copy-start.1 = (bf16[1,128,2048]{2,1,0:T(8,128)(2,1)S(1)}, bf16[1,128,2048]{2,1,0:T(8,128)(2,1)}, u32[]{:S(2)}) copy-start(bf16[1,128,2048]{2,1,0:T(8,128)(2,1)} %param.12) | copy-start | bytes 1572868
  0.0 52.0 %copy-start.3 = (f32[2048]{0:T(1024)S(1)}, f32[2048]{0:T(1024)}, u32[]{:S(2)}) copy-start(f32[2048]{0:T(1024)} %param.13) | copy-start | bytes 24580
  0.8 200.0 %copy-start.8 = (bf16[31,128]{1,0:T(8,128)(2,1)S(1)}, bf16[31,128]{1,0:T(8,128)(2,1)}, u32[]{:S(2)}) copy-start(bf16[31,128]{1,0:T(8,128)(2,1)} %param.16) | copy-start | bytes 23812
  2.1 198.3 %all-to-all-start = ((bf16[64,32,384]{2,1,0:T(8,128)(2,1)}), bf16[64,32,384]{2,1,0:T(8,128)(2,1)S(1)}, u32[]{:S(2)}, u32[]{:S(2)}) async-start(bf16[64,32,384]{2,1,0:T(8,128)(2,1)} %stack.12), calls=%async_computation | async-start | bytes 3145728 | tf_op jit(solution)/shard_map/all_to_all | solution.py:16
  202.6 14.5 %all-to-all-start.1 = ((f32[8,2,128]{2,1,0:T(2,128)}), f32[8,2,128]{2,1,0:T(2,128)S(1)}, u32[]{:S(2)}, u32[]{:S(2)}) async-start(f32[8,2,128]{2,1,0:T(2,128)} %broadcast_in_dim.5), calls=%async_computation.1 | async-start | bytes 16384 | tf_op jit(solution)/shard_map/all_to_all | solution.py:33
  219.6 7.5 copy-start.6
  219.7 7.5 copy-start.7
  219.7 389.8 %copy-start.2 = (bf16[1024,64]{0,1:T(8,128)(2,1)S(1)}, bf16[1024,64]{0,1:T(8,128)(2,1)}, u32[]{:S(2)}) copy-start(bf16[1024,64]{0,1:T(8,128)(2,1)} %param.22) | copy-start | bytes 393220
  219.7 377.1 %all-to-all-start.3 = ((bf16[64,32,1024]{2,1,0:T(8,128)(2,1)}), bf16[64,32,1024]{2,1,0:T(8,128)(2,1)}, u32[]{:S(2)}, u32[]{:S(2)}) async-start(bf16[64,32,1024]{2,1,0:T(8,128)(2,1)} %stack.16), calls=%async_computation.3 | async-start | bytes 8388608 | tf_op jit(solution)/shard_map/all_to_all | solution.py:16
  596.7 22.2 %all-to-all-start.2 = ((bf16[8,16,2048]{2,1,0:T(8,128)(2,1)}), bf16[8,16,2048]{2,1,0:T(8,128)(2,1)S(1)}, u32[]{:S(2)}, u32[]{:S(2)}) async-start(bf16[8,16,2048]{2,1,0:T(8,128)(2,1)} %bitcast.10), calls=%async_computation.2 | async-start | bytes 1048576 | tf_op jit(solution)/shard_map/all_to_all | solution.py:33
  621.4 7.9 copy-start.4
  621.4 377.6 %all-to-all-start.4 = ((bf16[64,32,1024]{2,1,0:T(8,128)(2,1)}), bf16[64,32,1024]{2,1,0:T(8,128)(2,1)}, u32[]{:S(2)}, u32[]{:S(2)}) async-start(bf16[64,32,1024]{2,1,0:T(8,128)(2,1)} %stack.17), calls=%async_computation.4 | async-start | bytes 8388608 | tf_op jit(solution)/shard_map/all_to_all | solution.py:16
  999.1 18.6 %copy-start.5 = (f32[256]{0:T(256)S(1)}, f32[256]{0:T(256)}, u32[]{:S(2)}) copy-start(f32[256]{0:T(256)} %param.23) | copy-start | bytes 3076
  1005.5 25.4 %all-to-all-start.5 = ((bf16[8,16,2048]{2,1,0:T(8,128)(2,1)}), bf16[8,16,2048]{2,1,0:T(8,128)(2,1)S(1)}, u32[]{:S(2)}, u32[]{:S(2)}) async-start(bf16[8,16,2048]{2,1,0:T(8,128)(2,1)} %bitcast.14), calls=%async_computation.5 | async-start | bytes 1048576 | tf_op jit(solution)/shard_map/all_to_all | solution.py:33
